TPU v7x, 128 devices: a whole 4x4x4 slice. The times are simulated.
128 devices in a mesh: ra: 16 (over z, y), cb: 8 (over x, core).
Axes of the slice: x: 4, y: 4, z: 4, core: 2. Of those that a mesh axis runs over, the one named last changes fastest.
Arguments:
- tokens: bfloat16 [1024, 4096], P(None, 'ra'), may hold values from -40 to 40
- norm_gain: float32 [4096], P('ra'), may hold values from 0.1 to 1.9
- gate_weight: bfloat16 [4096, 11264], P('ra', 'cb'), may hold values from -0.09375 to 0.09375
- up_weight: bfloat16 [4096, 11264], P('ra', 'cb'), may hold values from -0.09375 to 0.09375
- down_weight: bfloat16 [11264, 4096], P('cb', 'ra'), may hold values from -0.0546875 to 0.0546875
- out_gain: float32 [4096], P('ra'), may hold values from 0.1 to 1.9
Outputs:
- normed: bfloat16 [1024, 4096], P(None, 'ra')
All inputs are finite; a program needn't handle non-finite values.
Results may differ from a plain program's by a relative error of at most 0.0076.
Values may be sent and summed in bfloat16 or wider, within the bound.
A program may use at most 128 MiB of HBM per device.

v0:
```python
import functools

import jax
import jax.numpy as jnp
from jax import lax
from jax.experimental import pallas as pl
from jax.experimental.pallas import tpu as pltpu
from jax.sharding import PartitionSpec as P

D = 4096
EPS = 1e-06
MESH = pl.DeviceIdType.MESH
scope = jax.named_scope
F32 = jnp.float32
BF16 = jnp.bfloat16
T = 1024
H = 512
B = 128
W = 256
L = 128
K = 3

R = 112

S0 = 64
HALVES = ((0, S0), (S0, B))

JOBS = ((0, "z", True), (1, "z", True), (2, "z", True), (3, "z", True), (4, "y", False), (5, "y", False))

PASSED = 2

NEAR = (2, 1, 3)
EVERYONE = [(g, f, d, e) for g in range(4) for f in range(4) for d in range(4) for e in range(2)][1:]
EVERYONE.sort(key=lambda s: -sum(min(v, 4 - v) for v in s[:3]))


def mod4(v):
    return lax.rem(v + 4, 4)


def row_sums(v):
    sq = v * v
    hi = sq.astype(BF16)
    lo = (sq - hi.astype(F32)).astype(BF16)
    ones = jnp.ones((8, v.shape[1]), BF16)
    dims = (((1,), (1,)), ((), ()))
    out = lax.dot_general(ones, hi, dims, preferred_element_type=F32)
    return (out + lax.dot_general(ones, lo, dims, preferred_element_type=F32))[:1]


def as_columns(row):
    return jnp.transpose(jnp.broadcast_to(row, (L, L)), (1, 0))


def kernel(
    tok_h, gain_h, wg_h, wu_h, wd_h, ogain_h, out,
    tok, gain, wg, wu, wd, ogain, xg, xz, wb, wdb, part, zr, zs, rbuf, rdir, hall, hz, begun, psend, p1, p2, s1, s2, p3, p4,
    sq_s, sq_r, sq2_r, sq3_r, st2_s, st_all, sq_n,
    sent, head, loc, xa_rs, xb_rs, xc_rs, xz_rs, w_rs, f_rs, d_rs, df_rs, relay_rs, sum_rs, shown_rs, h_rs, hy_rs,
    p_rs, q_rs, t_rs, o_rs, of_rs,
):
    ra, cb = lax.axis_index("ra"), lax.axis_index("cb")
    z, y, x, c = ra // 4, lax.rem(ra, 4), cb // 2, lax.rem(cb, 2)

    def dev(dz=0, dy=0, dx=0, dc=0):
        return (mod4(z + dz) * 4 + mod4(y + dy), mod4(x + dx) * 2 + lax.rem(c + dc, 2))

    def rows(start, size):
        return pl.ds(pl.multiple_of(start, 8), size)

    sends = []

    def send(src, dst, rs, to):
        cp = pltpu.make_async_remote_copy(
            src_ref=src, dst_ref=dst, send_sem=sent, recv_sem=rs, device_id=to, device_id_type=MESH
        )
        cp.start()
        sends.append(cp)
        return cp

    def arrived(ref, sem):
        pltpu.make_async_copy(ref, ref, sem).wait()

    def local(src, dst, sem):
        cp = pltpu.make_async_copy(src, dst, sem)
        cp.start()
        return cp

    partners = [dev(dz=d) for d in NEAR] + [dev(dy=d) for d in NEAR] + [dev(dx=d) for d in NEAR] + [dev(dc=1)]
    bar = pltpu.get_barrier_semaphore()
    for p in partners:
        pl.semaphore_signal(bar, inc=1, device_id=p, device_id_type=MESH)

    mine = rows(c * H, H)
    first = [local(tok_h.at[mine, :], tok, head.at[0]), local(gain_h, gain, head.at[1])]
    heads = [
        local(src, dst, head.at[2 + i]) for i, (src, dst) in enumerate(((wg_h, wg), (wu_h, wu), (wd_h, wd), (ogain_h, ogain)))
    ]

    def tile0(yy):
        return jnp.minimum(3 * yy, 8)

    def cols(yy, k):
        return pl.ds(pl.multiple_of((tile0(yy) + k) * L, L), L)

    for k in range(K):
        own = cols(y if k < 2 else z, k)
        local(wg_h.at[:, own], wb.at[k, c, 0, :, :L], loc.at[k])
        local(wu_h.at[:, own], wb.at[k, c, 0, :, L:], loc.at[k])
    local_d = local(wd_h.at[pl.ds(tile0(y), K)], wdb.at[y, :, c], loc.at[K])

    for h in first:
        h.wait()
    xg[0] = (tok[...].astype(F32) * gain[...]).astype(BF16)
    with scope("barrier"):
        pl.semaphore_wait(bar, len(partners))

    quarter = rows(x * R, R)
    for d in NEAR:
        send(xg.at[0, quarter], xg.at[d, quarter], xa_rs.at[d - 1], dev(dy=d))
    for d in (1, 3):
        send(xg.at[0, 4 * R :], xg.at[d, 4 * R :], xb_rs.at[d - 1], dev(dy=d))
    near_z = {d: send(xg.at[0], xz.at[d - 1], xz_rs.at[d - 1], dev(dz=d)) for d in (1, 3)}
    for h in heads:
        h.wait()

    def send_columns(k):
        for d in NEAR:
            own, to = (mod4(y + d), dev(dy=d)) if k < 2 else (mod4(z + d), dev(dz=d))
            send(wg.at[:, cols(own, k)], wb.at[k, c, d, :, :L], w_rs.at[k, d - 1], to)
            send(wu.at[:, cols(own, k)], wb.at[k, c, d, :, L:], w_rs.at[k, d - 1], to)

    send_columns(0)
    send_columns(2)
    sq = row_sums(tok[...].astype(F32))
    for b in range(4):
        sq_s[b] = sq[:, b * L : (b + 1) * L]
    for d in NEAR:
        send(sq_s, sq_r.at[d - 1], q_rs.at[0], dev(dy=d))
    for d in (1, 3, 2):
        with scope(f"wait_xa#d={d}"):
            arrived(xg.at[d, quarter], xa_rs.at[d - 1])
        for e in NEAR:
            send(xg.at[d, quarter], xg.at[d, quarter], xc_rs, dev(dx=e))
    cut = 4 * R + (H - 4 * R) // 2
    for d, part_of in ((1, slice(4 * R, cut)), (3, slice(cut, H))):
        with scope(f"wait_xb#d={d}"):
            arrived(xg.at[d, 4 * R :], xb_rs.at[d - 1])
        send(xg.at[d, part_of], xg.at[2, part_of], xb_rs.at[1], dev(dy=d))
    send_columns(1)

    def send_rows(d, k0, k1):
        tiles = pl.ds(tile0(mod4(y + d)) + k0, k1 - k0)
        send(wd.at[tiles], wdb.at[y, k0:k1, c], d_rs.at[d - 1], dev(dy=d))

    for d in (1, 3):
        send_rows(d, 0, 1)
    with scope("wait_xz"):
        for d, half in ((1, slice(0, H // 2)), (3, slice(H // 2, H))):
            near_z[d].wait_recv()
            send(xz.at[d - 1, half], xz.at[1, half], xz_rs.at[1], dev(dz=d))
    def columns_of(k):
        with scope(f"wait_w#k={k}"):
            for d in NEAR:
                arrived(wb.at[k, c, d], w_rs.at[k, d - 1])
                send(wb.at[k, c, d], wb.at[k, c, d], f_rs.at[k], dev(dc=1))

    def along(axis, d):
        return (dev(dz=d), mod4(z + d)) if axis == "z" else (dev(dy=d), mod4(y + d))

    def block_of(at, r0=0, r1=B):
        return rows(at * B + r0, r1 - r0)

    def multiply(u):
        k, cc = u // 2, lax.rem(c + u % 2, 2)
        if u % 2:
            with scope(f"wait_f#k={k}"):
                arrived(wb.at[k, cc], f_rs.at[k])
        acc = jnp.zeros((H, 2 * L), F32)
        for d in range(4):
            xs = xz[d - 1] if u >= 4 and d else xg[d]
            acc = acc + jnp.dot(xs, wb[k, cc, d], preferred_element_type=F32)
        part[u] = acc.astype(BF16)

    half = B // 2

    def start(u):
        _, axis, through = JOBS[u]
        if not through:
            for d in NEAR:
                to, at = along(axis, d)
                send(part.at[u, block_of(at)], rdir.at[u, d - 1], sum_rs.at[u], to)
            return
        far = along(axis, 2)[1]
        (up1, above), (dn1, below) = along(axis, 1), along(axis, 3)
        send(part.at[u, block_of(far, 0, half)], zr.at[u, 0], relay_rs.at[u, 0], up1)
        send(part.at[u, block_of(far, half, B)], zr.at[u, 1], relay_rs.at[u, 1], dn1)
        send(part.at[u, block_of(above, half, B)], rbuf.at[u, 0, half:], sum_rs.at[u], up1)
        send(part.at[u, block_of(below, 0, half)], rbuf.at[u, 1, :half], sum_rs.at[u], dn1)

    def add(u):
        _, axis, _ = JOBS[u]
        for side, d, a, b in ((0, 1, 0, half), (1, 3, half, B)):
            to, at = along(axis, d)
            with scope(f"wait_relay#u={u}"):
                arrived(zr.at[u, side], relay_rs.at[u, side])
            zs[u, side] = (part[u, block_of(at, a, b), :].astype(F32) + zr[u, side].astype(F32)).astype(BF16)
            send(zs.at[u, side], rbuf.at[u, side, a:b], sum_rs.at[u], to)

    def core_of(u):
        return lax.rem(c + u % 2, 2)

    def finish(u):
        _, axis, through = JOBS[u]
        came = rbuf if through else rdir
        with scope(f"wait_sum#u={u}"):
            arrived(came.at[u], sum_rs.at[u])
        total = part[u, block_of(along(axis, 0)[1]), :].astype(F32)
        for d in range(2 if through else 3):
            total = total + came[u, d].astype(F32)
        scale = inv if axis == "z" else inv_y
        gate, up = total[:, :L] * scale, total[:, L:] * scale
        hid = gate / (1.0 + jnp.exp(-gate)) * up
        if u < 2:
            hid = jnp.where(y == 3, jnp.zeros_like(hid), hid)
        if axis == "z":
            lanes = pl.ds(pl.multiple_of((u // 2 * 2 + core_of(u)) * L, L), L)
            hall[z, :, lanes] = hid.astype(BF16)
            block = hall.at[z, :, lanes]
        else:
            lanes = pl.ds(pl.multiple_of(core_of(u) * L, L), L)
            hz[z, :, lanes] = hid.astype(BF16)
            block = hz.at[z, :, lanes]
        if u < PASSED:
            send(block, block, shown_rs.at[u, 0], dev(dz=1))
            send(block, block, shown_rs.at[u, 1], dev(dz=3))
            return
        for d in NEAR:
            send(block, block, h_rs.at[u // 4], dev(dz=d))

    def pass_on(u):
        lanes = pl.ds(pl.multiple_of((u // 2 * 2 + core_of(u)) * L, L), L)
        for side, to, dz, a, b in ((0, 1, 3, 0, half), (1, 3, 1, half, B)):
            with scope(f"wait_shown#u={u}"):
                arrived(hall.at[mod4(z + dz), :, lanes], shown_rs.at[u, side])
            block = hall.at[mod4(z + dz), a:b, lanes]
            send(block, block, h_rs.at[0], dev(dz=to))

    for k in range(K):
        arrived(wb.at[k, c, 0], loc.at[k])
        send(wb.at[k, c, 0], wb.at[k, c, 0], f_rs.at[k], dev(dc=1))
    local_d.wait()
    send(wdb.at[y, :, c], wdb.at[y, :, c], df_rs, dev(dc=1))
    columns_of(0)
    with scope("wait_xc"):
        arrived(xg.at[1:, : 3 * R], xc_rs)
    with scope("wait_xb2"):
        arrived(xg.at[2, 4 * R :], xb_rs.at[1])
    multiply(0)
    start(0)
    columns_of(2)
    with scope("wait_sq"):
        arrived(sq_r, q_rs.at[0])
    for b in range(4):
        st2_s[b] = sq_s[b] + sq_r[0, b] + sq_r[1, b] + sq_r[2, b]
    for d in NEAR:
        send(st2_s.at[mod4(z + d)], sq2_r.at[d - 1], q_rs.at[1], dev(dz=d))
        send(st2_s.at[y], sq3_r.at[d - 1], q_rs.at[2], dev(dz=d))
    multiply(1)
    start(1)
    with scope("wait_xz2"):
        arrived(xz.at[1], xz_rs.at[1])
    multiply(4)
    start(4)
    multiply(5)
    start(5)
    for d in NEAR:
        send_rows(d, 0 if d == 2 else 1, K)
    add(0)
    columns_of(1)
    add(1)
    multiply(2)
    start(2)
    multiply(3)
    start(3)
    with scope("wait_sq2"):
        arrived(sq2_r, q_rs.at[1])
        arrived(sq3_r, q_rs.at[2])
    inv = as_columns(lax.rsqrt((st2_s[z] + sq2_r[0] + sq2_r[1] + sq2_r[2]) / D + EPS))
    inv_y = as_columns(lax.rsqrt((st2_s[y] + sq3_r[0] + sq3_r[1] + sq3_r[2]) / D + EPS))
    finish(0)
    finish(1)
    add(2)
    finish(4)
    add(3)
    finish(5)
    finish(2)
    pass_on(0)
    pass_on(1)
    with scope("wait_d2"):
        arrived(wdb.at[0, :, c], d_rs.at[1])
        send(wdb.at[mod4(y - 2), :, c], wdb.at[mod4(y - 2), :, c], df_rs, dev(dc=1))
    finish(3)
    with scope("wait_hz"):
        arrived(hz.at[:3], h_rs.at[1])
    last = slice(4 * L, 6 * L)
    for i, (r0, r1) in enumerate(HALVES):
        for d in NEAR:
            send(hz.at[mod4(y + d), r0:r1], hall.at[y, r0:r1, last], hy_rs.at[i], dev(dy=d))
    hall[y, :, last] = hz[y]
    with scope("wait_d"):
        for d in (1, 3):
            arrived(wdb.at[0, :, c], d_rs.at[d - 1])
            block = wdb.at[mod4(y - d), :, c]
            send(block, block, df_rs, dev(dc=1))
    with scope("wait_df"):
        arrived(wdb.at[:, :, c], df_rs)

    with scope("wait_h"):
        arrived(hall.at[:2, :, : 4 * L], h_rs.at[0])
    for yy in range(4):
        w = wdb[yy, :2].reshape(4 * L, W)
        begun[yy] = jnp.dot(hall[:, :, : 4 * L].reshape(H, 4 * L), w, preferred_element_type=F32).reshape(4, B, W)
    for i, (r0, r1) in enumerate(HALVES):
        with scope(f"wait_hy#i={i}"):
            arrived(hall.at[:3, r0:r1, last], hy_rs.at[i])
        mid = (r0 + r1) // 2
        a, b = slice(r0, mid), slice(mid, r1)
        for dy in (2, 1, 3, 0):
            yy = mod4(y + dy)
            hid = hall[:, r0:r1, 4 * L :].reshape(4 * (r1 - r0), 2 * L)
            acc = jnp.dot(hid, wdb[yy, 2].reshape(2 * L, W), preferred_element_type=F32)
            psend[yy, :, r0:r1] = (begun[yy, :, r0:r1] + acc.reshape(4, r1 - r0, W)).astype(BF16)
            if dy:
                send(psend.at[yy, :, a], p1.at[dy - 1, :, a], p_rs.at[i, 0], dev(dy=dy))
            for dx in NEAR:
                send(psend.at[yy, mod4(x + dx), b], p2.at[dx - 1, yy, b], p_rs.at[i, 1], dev(dx=dx))
    for i, (r0, r1) in enumerate(HALVES):
        mid = (r0 + r1) // 2
        a, b = slice(r0, mid), slice(mid, r1)
        with scope(f"wait_p1#i={i}"):
            arrived(p1.at[:, :, a], p_rs.at[i, 0])
        for xx in range(4):
            v = psend[y, xx, a].astype(F32)
            for d in range(3):
                v = v + p1[d, xx, a].astype(F32)
            s1[xx, a] = v.astype(BF16)
        for d in NEAR:
            send(s1.at[mod4(x + d), a], p3.at[d - 1, a], p_rs.at[i, 2], dev(dx=d))
        with scope(f"wait_p2#i={i}"):
            arrived(p2.at[:, :, b], p_rs.at[i, 1])
        for yy in range(4):
            v = psend[yy, x, b].astype(F32)
            for d in range(3):
                v = v + p2[d, yy, b].astype(F32)
            s2[yy, b] = v.astype(BF16)
        for d in NEAR:
            send(s2.at[mod4(y + d), b], p4.at[d - 1, b], p_rs.at[i, 3], dev(dy=d))
    pieces = []
    for i, (r0, r1) in enumerate(HALVES):
        mid = (r0 + r1) // 2
        a, b = slice(r0, mid), slice(mid, r1)
        with scope(f"wait_p3#i={i}"):
            arrived(p3.at[:, a], p_rs.at[i, 2])
        v1 = s1[x, a].astype(F32)
        for d in range(3):
            v1 = v1 + p3[d, a].astype(F32)
        with scope(f"wait_p4#i={i}"):
            arrived(p4.at[:, b], p_rs.at[i, 3])
        v2 = s2[y, b].astype(F32)
        for d in range(3):
            v2 = v2 + p4[d, b].astype(F32)
        piece = rows(c * H + x * B + r0, r1 - r0)
        pieces.append(0.5 * tok[rows(x * B + r0, r1 - r0), :].astype(F32) + jnp.concatenate([v1, v2], axis=0))
        out[piece, :] = pieces[i].astype(BF16)
        if i == 0:
            for d in NEAR:
                send(out.at[piece, :], out.at[piece, :], o_rs.at[i, d - 1], dev(dx=d))
    stream = jnp.concatenate(pieces, axis=0)
    mine = 2 * x + c
    st_all[mine, 0] = row_sums(stream)
    for dz, f, d, e in EVERYONE:
        send(st_all.at[mine, 0], st_all.at[mine, 4 * dz + f], t_rs, dev(dz=dz, dy=f, dx=d, dc=e))
    for d in NEAR:
        send(out.at[piece, :], out.at[piece, :], o_rs.at[1, d - 1], dev(dx=d))
    for i, (r0, r1) in enumerate(HALVES):
        with scope(f"wait_o#i={i}"):
            for d in (0, 1, 3, 2):
                block = out.at[rows(c * H + mod4(x - d) * B + r0, r1 - r0), :]
                if d:
                    arrived(block, o_rs.at[i, d - 1])
                send(block, block, of_rs, dev(dc=1))
    with scope("wait_of"):
        arrived(out.at[:H], of_rs)
    with scope("wait_st2"):
        arrived(sq_n.at[: len(EVERYONE)], t_rs)
    with scope("wait_sends"):
        for s in sends:
            s.wait_send()
    for xx in range(4):
        for cc in range(2):
            total = jnp.sum(st_all[2 * xx + cc], axis=0)
            factor = as_columns(lax.rsqrt(total / D + EPS))
            r = slice(cc * H + xx * B, cc * H + (xx + 1) * B)
            for h in range(2):
                lanes = slice(h * L, (h + 1) * L)
                out[r, lanes] = (out[r, lanes].astype(F32) * factor * ogain[:, lanes]).astype(BF16)


def body(tokens, norm_gain, gate_weight, up_weight, down_weight, out_gain):
    dma = pltpu.SemaphoreType.DMA
    hbm = pl.BlockSpec(memory_space=pltpu.HBM)
    operands = (
        tokens,
        norm_gain.reshape(1, W),
        gate_weight,
        up_weight,
        down_weight.reshape(11, L, W),
        out_gain.reshape(1, W),
    )
    return pl.pallas_call(
        kernel,
        out_shape=jax.ShapeDtypeStruct((T, W), BF16),
        in_specs=[hbm] * 6,
        out_specs=pl.BlockSpec(memory_space=pltpu.VMEM),
        scratch_shapes=[
            pltpu.VMEM((H, W), BF16),
            pltpu.VMEM((1, W), F32),
            pltpu.VMEM((W, 11 * L), BF16),
            pltpu.VMEM((W, 11 * L), BF16),
            pltpu.VMEM((11, L, W), BF16),
            pltpu.VMEM((1, W), F32),
            pltpu.VMEM((4, H, W), BF16),
            pltpu.VMEM((3, H, W), BF16),
            pltpu.VMEM((K, 2, 4, W, 2 * L), BF16),
            pltpu.VMEM((4, K, 2, L, W), BF16),
            pltpu.VMEM((2 * K, H, 2 * L), BF16),
            pltpu.VMEM((2 * K, 2, B // 2, 2 * L), BF16),
            pltpu.VMEM((2 * K, 2, B // 2, 2 * L), BF16),
            pltpu.VMEM((2 * K, 2, B, 2 * L), BF16),
            pltpu.VMEM((2 * K, 3, B, 2 * L), BF16),
            pltpu.VMEM((4, B, 2 * K * L), BF16),
            pltpu.VMEM((4, B, 2 * L), BF16),
            pltpu.VMEM((4, 4, B, W), F32),
            pltpu.VMEM((4, 4, B, W), BF16),
            pltpu.VMEM((3, 4, B, W), BF16),
            pltpu.VMEM((3, 4, B, W), BF16),
            pltpu.VMEM((4, B, W), BF16),
            pltpu.VMEM((4, B, W), BF16),
            pltpu.VMEM((3, B, W), BF16),
            pltpu.VMEM((3, B, W), BF16),
            pltpu.VMEM((4, 1, L), F32),
            pltpu.VMEM((3, 4, 1, L), F32),
            pltpu.VMEM((3, 1, L), F32),
            pltpu.VMEM((3, 1, L), F32),
            pltpu.VMEM((4, 1, L), F32),
            pltpu.VMEM((8, 16, 1, L), F32),
            pltpu.VMEM((128, 1, L), F32),
            dma,
            dma((6,)),
            dma((K + 1,)),
            dma((3,)), dma((3,)), dma, dma((3,)),
            dma((K, 3)), dma((K,)), dma((3,)), dma,
            dma((len(JOBS), 2)), dma((len(JOBS),)),
            dma((PASSED, 2)), dma((2,)), dma((2,)),
            dma((2, 4)), dma((3,)), dma,
            dma((2, 3)), dma,
        ],
        compiler_params=pltpu.CompilerParams(
            collective_id=0, has_side_effects=True, vmem_limit_bytes=40 * 1024 * 1024
        ),
    )(*[pltpu.with_memory_space_constraint(a, pltpu.HBM) for a in operands])


def solution(mesh):
    placed = (P(None, "ra"), P("ra"), P("ra", "cb"), P("ra", "cb"), P("cb", "ra"), P("ra"))
    return jax.shard_map(body, mesh=mesh, in_specs=placed, out_specs=P(None, "ra"), check_vma=False)
```

profile of v0, /device:TPU:1, one launch (start us, length us, event | category | flops | bytes accessed | tf_op | source)
XLA Modules:
  0.0 62.3 jit_solution(8724151953818473864)
XLA Ops:
  0.0 61.5 %shard_map.64 = bf16[1024,256]{1,0:T(8,128)(2,1)S(1)} custom-call(bf16[1024,256]{1,0:T(8,128)(2,1)} %tok_h.1, f32[1,256]{1,0:T(1,128)} %bitcast.4, bf16[256,1408]{1,0:T(8,128)(2,1)} %wg_h.1, bf16[256,1408]{1,0:T(8,128)(2,1)} %wu_h.1, bf16[11,128,256]{2,1,0:T(8,128)(2,1)} %bitcast.3, f32[1,256]{1,0:T(1,128)} %bitcast.5), custom_call_target="tpu_custom_call" | custom-call | tf_op jit(solution)/shard_map/pallas_call | solution.py:421
  61.5 0.8 %copy.8 = bf16[1024,256]{1,0:T(8,128)(2,1)} copy(bf16[1024,256]{1,0:T(8,128)(2,1)S(1)} %shard_map.64) | data formatting | bytes 1048576
where the time goes:
time: 62.5 us; the launch traced here: 62.3 us
  Pallas kernels  61.5 us (98%)
  local copies, waits for them, and re-layouts  0.8 us (1%)
    pallas_call x1, Pallas kernels, body(): pl.pallas_call(kernel, out_shape=jax.ShapeDtypeStruct((T, W), BF16), in_s...  61.5 us

commit v1 on v0

--- a/solution.py
+++ b/solution.py
@@ -21,6 +21,7 @@
 K = 3
 
 R = 112
+RZ = 32
 
 S0 = 64
 HALVES = ((0, S0), (S0, B))
@@ -56,7 +57,7 @@
     tok_h, gain_h, wg_h, wu_h, wd_h, ogain_h, out,
     tok, gain, wg, wu, wd, ogain, xg, xz, wb, wdb, part, zr, zs, rbuf, rdir, hall, hz, begun, psend, p1, p2, s1, s2, p3, p4,
     sq_s, sq_r, sq2_r, sq3_r, st2_s, st_all, sq_n,
-    sent, head, loc, xa_rs, xb_rs, xc_rs, xz_rs, w_rs, f_rs, d_rs, df_rs, relay_rs, sum_rs, shown_rs, h_rs, hy_rs,
+    sent, head, loc, xa_rs, xb_rs, xc_rs, xz_rs, xza_rs, xzc_rs, w_rs, f_rs, d_rs, df_rs, relay_rs, sum_rs, shown_rs, h_rs, hy_rs,
     p_rs, q_rs, t_rs, o_rs, of_rs,
 ):
     ra, cb = lax.axis_index("ra"), lax.axis_index("cb")
@@ -120,7 +121,10 @@
         send(xg.at[0, quarter], xg.at[d, quarter], xa_rs.at[d - 1], dev(dy=d))
     for d in (1, 3):
         send(xg.at[0, 4 * R :], xg.at[d, 4 * R :], xb_rs.at[d - 1], dev(dy=d))
-    near_z = {d: send(xg.at[0], xz.at[d - 1], xz_rs.at[d - 1], dev(dz=d)) for d in (1, 3)}
+    quarter_z = rows(x * RZ, RZ)
+    for d in NEAR:
+        send(xg.at[0, quarter_z], xz.at[d - 1, quarter_z], xza_rs.at[d - 1], dev(dz=d))
+    near_z = {d: send(xg.at[0, 4 * RZ :], xz.at[d - 1, 4 * RZ :], xz_rs.at[d - 1], dev(dz=d)) for d in (1, 3)}
     for h in heads:
         h.wait()
 
@@ -153,10 +157,14 @@
         tiles = pl.ds(tile0(mod4(y + d)) + k0, k1 - k0)
         send(wd.at[tiles], wdb.at[y, k0:k1, c], d_rs.at[d - 1], dev(dy=d))
 
-    for d in (1, 3):
-        send_rows(d, 0, 1)
+    with scope("wait_xza"):
+        for d in (1, 3, 2):
+            block = xz.at[d - 1, quarter_z]
+            arrived(block, xza_rs.at[d - 1])
+            for e in NEAR:
+                send(block, block, xzc_rs, dev(dx=e))
     with scope("wait_xz"):
-        for d, half in ((1, slice(0, H // 2)), (3, slice(H // 2, H))):
+        for d, half in ((1, slice(4 * RZ, 2 * RZ + H // 2)), (3, slice(2 * RZ + H // 2, H))):
             near_z[d].wait_recv()
             send(xz.at[d - 1, half], xz.at[1, half], xz_rs.at[1], dev(dz=d))
     def columns_of(k):
@@ -269,13 +277,15 @@
     multiply(1)
     start(1)
     with scope("wait_xz2"):
-        arrived(xz.at[1], xz_rs.at[1])
+        arrived(xz.at[1, 4 * RZ :], xz_rs.at[1])
+    with scope("wait_xzc"):
+        arrived(xz.at[:, : 3 * RZ], xzc_rs)
     multiply(4)
     start(4)
     multiply(5)
     start(5)
     for d in NEAR:
-        send_rows(d, 0 if d == 2 else 1, K)
+        send_rows(d, 0, K)
     add(0)
     columns_of(1)
     add(1)
@@ -459,7 +469,7 @@
             dma,
             dma((6,)),
             dma((K + 1,)),
-            dma((3,)), dma((3,)), dma, dma((3,)),
+            dma((3,)), dma((3,)), dma, dma((3,)), dma((3,)), dma,
             dma((K, 3)), dma((K,)), dma((3,)), dma,
             dma((len(JOBS), 2)), dma((len(JOBS),)),
             dma((PASSED, 2)), dma((2,)), dma((2,)),

time: 62.5 us -> 62.1 us (level)
  no operation moved by 1% of the time
where the time goes in v1:
time: 62.1 us; the launch traced here: 62 us
  Pallas kernels  61.2 us (99%)
  local copies, waits for them, and re-layouts  0.8 us (1%)
    pallas_call x1, Pallas kernels, body(): pl.pallas_call(kernel, out_shape=jax.ShapeDtypeStruct((T, W), BF16), in_s...  61.2 us

profile of v1, /device:TPU:1, one launch (start us, length us, event | category | flops | bytes accessed | tf_op | source)
XLA Modules:
  0.0 62.0 jit_solution(4114830852172268346)
XLA Ops:
  0.0 61.2 %shard_map.64 = bf16[1024,256]{1,0:T(8,128)(2,1)S(1)} custom-call(bf16[1024,256]{1,0:T(8,128)(2,1)} %tok_h.1, f32[1,256]{1,0:T(1,128)} %bitcast.4, bf16[256,1408]{1,0:T(8,128)(2,1)} %wg_h.1, bf16[256,1408]{1,0:T(8,128)(2,1)} %wu_h.1, bf16[11,128,256]{2,1,0:T(8,128)(2,1)} %bitcast.3, f32[1,256]{1,0:T(1,128)} %bitcast.5), custom_call_target="tpu_custom_call" | custom-call | tf_op jit(solution)/shard_map/pallas_call | solution.py:431
  61.2 0.8 %copy.8 = bf16[1024,256]{1,0:T(8,128)(2,1)} copy(bf16[1024,256]{1,0:T(8,128)(2,1)S(1)} %shard_map.64) | data formatting | bytes 1048576

commit v2 on v1

--- a/solution.py
+++ b/solution.py
@@ -93,9 +93,9 @@
         pl.semaphore_signal(bar, inc=1, device_id=p, device_id_type=MESH)
 
     mine = rows(c * H, H)
-    first = [local(tok_h.at[mine, :], tok, head.at[0]), local(gain_h, gain, head.at[1])]
+    first = [local(tok_h.at[mine, :], tok, head.at[0]), local(gain_h, gain, head.at[0])]
     heads = [
-        local(src, dst, head.at[2 + i]) for i, (src, dst) in enumerate(((wg_h, wg), (wu_h, wu), (wd_h, wd), (ogain_h, ogain)))
+        local(src, dst, head.at[1]) for src, dst in ((wg_h, wg), (wu_h, wu), (wd_h, wd), (ogain_h, ogain))
     ]
 
     def tile0(yy):
@@ -123,7 +123,7 @@
         send(xg.at[0, 4 * R :], xg.at[d, 4 * R :], xb_rs.at[d - 1], dev(dy=d))
     quarter_z = rows(x * RZ, RZ)
     for d in NEAR:
-        send(xg.at[0, quarter_z], xz.at[d - 1, quarter_z], xza_rs.at[d - 1], dev(dz=d))
+        send(xg.at[0, quarter_z], xz.at[d - 1, quarter_z], xza_rs, dev(dz=d))
     near_z = {d: send(xg.at[0, 4 * RZ :], xz.at[d - 1, 4 * RZ :], xz_rs.at[d - 1], dev(dz=d)) for d in (1, 3)}
     for h in heads:
         h.wait()
@@ -158,11 +158,9 @@
         send(wd.at[tiles], wdb.at[y, k0:k1, c], d_rs.at[d - 1], dev(dy=d))
 
     with scope("wait_xza"):
-        for d in (1, 3, 2):
-            block = xz.at[d - 1, quarter_z]
-            arrived(block, xza_rs.at[d - 1])
-            for e in NEAR:
-                send(block, block, xzc_rs, dev(dx=e))
+        arrived(xz.at[:, quarter_z], xza_rs)
+        for e in NEAR:
+            send(xz.at[:, quarter_z], xz.at[:, quarter_z], xzc_rs, dev(dx=e))
     with scope("wait_xz"):
         for d, half in ((1, slice(4 * RZ, 2 * RZ + H // 2)), (3, slice(2 * RZ + H // 2, H))):
             near_z[d].wait_recv()
@@ -341,10 +339,10 @@
             hid = hall[:, r0:r1, 4 * L :].reshape(4 * (r1 - r0), 2 * L)
             acc = jnp.dot(hid, wdb[yy, 2].reshape(2 * L, W), preferred_element_type=F32)
             psend[yy, :, r0:r1] = (begun[yy, :, r0:r1] + acc.reshape(4, r1 - r0, W)).astype(BF16)
+            for dx in NEAR:
+                send(psend.at[yy, mod4(x + dx), b], p2.at[dx - 1, yy, b], p_rs.at[i, 1], dev(dx=dx))
             if dy:
                 send(psend.at[yy, :, a], p1.at[dy - 1, :, a], p_rs.at[i, 0], dev(dy=dy))
-            for dx in NEAR:
-                send(psend.at[yy, mod4(x + dx), b], p2.at[dx - 1, yy, b], p_rs.at[i, 1], dev(dx=dx))
     for i, (r0, r1) in enumerate(HALVES):
         mid = (r0 + r1) // 2
         a, b = slice(r0, mid), slice(mid, r1)
@@ -467,11 +465,11 @@
             pltpu.VMEM((8, 16, 1, L), F32),
             pltpu.VMEM((128, 1, L), F32),
             dma,
-            dma((6,)),
+            dma((2,)),
             dma((K + 1,)),
-            dma((3,)), dma((3,)), dma, dma((3,)), dma((3,)), dma,
+            dma((3,)), dma((3,)), dma, dma((3,)), dma, dma,
             dma((K, 3)), dma((K,)), dma((3,)), dma,
-            dma((len(JOBS), 2)), dma((len(JOBS),)),
+            dma((4, 2)), dma((len(JOBS),)),
             dma((PASSED, 2)), dma((2,)), dma((2,)),
             dma((2, 4)), dma((3,)), dma,
             dma((2, 3)), dma,

time: 62.1 us -> 62 us (level)
  no operation moved by 1% of the time
where the time goes in v2:
time: 62 us; the launch traced here: 61.9 us
  Pallas kernels  61.1 us (99%)
  local copies, waits for them, and re-layouts  0.8 us (1%)
    pallas_call x1, Pallas kernels, body(): pl.pallas_call(kernel, out_shape=jax.ShapeDtypeStruct((T, W), BF16), in_s...  61.1 us

profile of v2, /device:TPU:1, one launch (start us, length us, event | category | flops | bytes accessed | tf_op | source)
XLA Modules:
  0.0 61.9 jit_solution(6357635280601378351)
XLA Ops:
  0.0 61.1 %shard_map.64 = bf16[1024,256]{1,0:T(8,128)(2,1)S(1)} custom-call(bf16[1024,256]{1,0:T(8,128)(2,1)} %tok_h.1, f32[1,256]{1,0:T(1,128)} %bitcast.4, bf16[256,1408]{1,0:T(8,128)(2,1)} %wg_h.1, bf16[256,1408]{1,0:T(8,128)(2,1)} %wu_h.1, bf16[11,128,256]{2,1,0:T(8,128)(2,1)} %bitcast.3, f32[1,256]{1,0:T(1,128)} %bitcast.5), custom_call_target="tpu_custom_call" | custom-call | tf_op jit(solution)/shard_map/pallas_call | solution.py:429
  61.1 0.8 %copy.8 = bf16[1024,256]{1,0:T(8,128)(2,1)} copy(bf16[1024,256]{1,0:T(8,128)(2,1)S(1)} %shard_map.64) | data formatting | bytes 1048576

commit v3 on v2

--- a/solution.py
+++ b/solution.py
@@ -54,7 +54,7 @@
 
 
 def kernel(
-    tok_h, gain_h, wg_h, wu_h, wd_h, ogain_h, out,
+    tok_h, gain_h, wg_h, wu_h, wd_h, ogain_h, out, scale,
     tok, gain, wg, wu, wd, ogain, xg, xz, wb, wdb, part, zr, zs, rbuf, rdir, hall, hz, begun, psend, p1, p2, s1, s2, p3, p4,
     sq_s, sq_r, sq2_r, sq3_r, st2_s, st_all, sq_n,
     sent, head, loc, xa_rs, xb_rs, xc_rs, xz_rs, xza_rs, xzc_rs, w_rs, f_rs, d_rs, df_rs, relay_rs, sum_rs, shown_rs, h_rs, hy_rs,
@@ -412,7 +412,7 @@
             r = slice(cc * H + xx * B, cc * H + (xx + 1) * B)
             for h in range(2):
                 lanes = slice(h * L, (h + 1) * L)
-                out[r, lanes] = (out[r, lanes].astype(F32) * factor * ogain[:, lanes]).astype(BF16)
+                scale[r, lanes] = factor * ogain[:, lanes]
 
 
 def body(tokens, norm_gain, gate_weight, up_weight, down_weight, out_gain):
@@ -426,11 +426,11 @@
         down_weight.reshape(11, L, W),
         out_gain.reshape(1, W),
     )
-    return pl.pallas_call(
+    stream, scale = pl.pallas_call(
         kernel,
-        out_shape=jax.ShapeDtypeStruct((T, W), BF16),
+        out_shape=(jax.ShapeDtypeStruct((T, W), BF16), jax.ShapeDtypeStruct((T, W), F32)),
         in_specs=[hbm] * 6,
-        out_specs=pl.BlockSpec(memory_space=pltpu.VMEM),
+        out_specs=(pl.BlockSpec(memory_space=pltpu.VMEM),) * 2,
         scratch_shapes=[
             pltpu.VMEM((H, W), BF16),
             pltpu.VMEM((1, W), F32),
@@ -478,6 +478,7 @@
             collective_id=0, has_side_effects=True, vmem_limit_bytes=40 * 1024 * 1024
         ),
     )(*[pltpu.with_memory_space_constraint(a, pltpu.HBM) for a in operands])
+    return (stream.astype(F32) * scale).astype(BF16)
 
 
 def solution(mesh):

time: 62 us -> 62.1 us (level)
  other arithmetic: 0 us -> 0.91 us
  local copies, waits for them, and re-layouts: 0.8 us -> 0 us
    convert_element_type x0 -> x1, other arithmetic: none -> 0.91 us  [body(): return (stream.astype(F32) * scale).astype(BF16)]
    unnamed x1 -> x0, local copies, waits for them, and re-layouts: 0.8 us -> none
where the time goes in v3:
time: 62.1 us; the launch traced here: 62 us
  Pallas kernels  61.1 us (98%)
  other arithmetic  0.91 us (1%)
    pallas_call x1, Pallas kernels, body(): pl.pallas_call(kernel, out_shape=(jax.ShapeDtypeStruct((T, W), BF16), jax...  61.1 us

profile of v3, /device:TPU:1, one launch (start us, length us, event | category | flops | bytes accessed | tf_op | source)
XLA Modules:
  0.0 62.0 jit_solution(1479831957882716931)
XLA Ops:
  0.0 61.1 %shard_map.64 = (bf16[1024,256]{1,0:T(8,128)(2,1)S(1)}, f32[1024,256]{1,0:T(8,128)S(1)}) custom-call(bf16[1024,256]{1,0:T(8,128)(2,1)} %tok_h.1, f32[1,256]{1,0:T(1,128)} %bitcast.4, bf16[256,1408]{1,0:T(8,128)(2,1)} %wg_h.1, bf16[256,1408]{1,0:T(8,128)(2,1)} %wu_h.1, bf16[11,128,256]{2,1,0:T(8,128)(2,1)} %bitcast.3, f32[1,256]{1,0:T(1,128)} %bitcast.5), custom_call_target="tpu_custom_call" | custom-call | tf_op jit(solution)/shard_map/pallas_call | solution.py:429
  61.1 0.9 %multiply_convert_fusion = bf16[1024,256]{1,0:T(8,128)(2,1)} fusion(f32[1024,256]{1,0:T(8,128)S(1)} %get-tuple-element.8, bf16[1024,256]{1,0:T(8,128)(2,1)S(1)} %get-tuple-element.7), kind=kLoop, calls=%fused_computation | loop fusion | flops 786432 | bytes 2097152 | tf_op jit(solution)/shard_map/convert_element_type | solution.py:481

commit v4 on v2

--- a/solution.py
+++ b/solution.py
@@ -20,7 +20,7 @@
 L = 128
 K = 3
 
-R = 112
+R = 104
 RZ = 32
 
 S0 = 64

time: 62 us -> 62.4 us (level)
  no operation moved by 1% of the time
where the time goes in v4:
time: 62.4 us; the launch traced here: 62.3 us
  Pallas kernels  61.5 us (99%)
  local copies, waits for them, and re-layouts  0.8 us (1%)
    pallas_call x1, Pallas kernels, body(): pl.pallas_call(kernel, out_shape=jax.ShapeDtypeStruct((T, W), BF16), in_s...  61.5 us

profile of v4, /device:TPU:1, one launch (start us, length us, event | category | flops | bytes accessed | tf_op | source)
XLA Modules:
  0.0 62.3 jit_solution(10009929253400737026)
XLA Ops:
  0.0 61.5 %shard_map.64 = bf16[1024,256]{1,0:T(8,128)(2,1)S(1)} custom-call(bf16[1024,256]{1,0:T(8,128)(2,1)} %tok_h.1, f32[1,256]{1,0:T(1,128)} %bitcast.4, bf16[256,1408]{1,0:T(8,128)(2,1)} %wg_h.1, bf16[256,1408]{1,0:T(8,128)(2,1)} %wu_h.1, bf16[11,128,256]{2,1,0:T(8,128)(2,1)} %bitcast.3, f32[1,256]{1,0:T(1,128)} %bitcast.5), custom_call_target="tpu_custom_call" | custom-call | tf_op jit(solution)/shard_map/pallas_call | solution.py:429
  61.5 0.8 %copy.8 = bf16[1024,256]{1,0:T(8,128)(2,1)} copy(bf16[1024,256]{1,0:T(8,128)(2,1)S(1)} %shard_map.64) | data formatting | bytes 1048576
